TPU v7x, 32 devices: a whole 2x2x4 slice. The times are simulated.
32 devices in a mesh: fs: 4 (over y, x), tp: 8 (over z, core).
Axes of the slice: x: 2, y: 2, z: 4, core: 2. Of those that a mesh axis runs over, the one named last changes fastest.
Arguments:
- normed_inputs: bfloat16 [4096, 4096], P('fs', 'tp'), may hold values from -6 to 6
- query_upstream: bfloat16 [4096, 4096], P('fs', 'tp'), may hold values from -0.125 to 0.125
- key_upstream: bfloat16 [4096, 1024], P('fs', 'tp'), may hold values from -0.09375 to 0.09375
- head_outputs: bfloat16 [4096, 4096], P('fs', 'tp'), may hold values from -6 to 6
- branch_upstream: bfloat16 [4096, 4096], P('fs', 'tp'), may hold values from -0.125 to 0.125
- query_master: float32 [4096, 4096], P('fs', 'tp'), may hold values from -0.09375 to 0.09375
- key_master: float32 [4096, 1024], P('fs', 'tp'), may hold values from -0.09375 to 0.09375
- branch_master: float32 [4096, 4096], P('fs', 'tp'), may hold values from -0.09375 to 0.09375
- query_basis: bfloat16 [4096, 128], replicated, may hold values from -0.09375 to 0.09375
- key_basis: bfloat16 [4096, 128], replicated, may hold values from -0.09375 to 0.09375
- branch_basis: bfloat16 [4096, 128], replicated, may hold values from -0.09375 to 0.09375
- query_first: float32 [128, 4096], P(None, 'tp'), may hold values from -0.75 to 0.75
- query_second: float32 [128, 4096], P(None, 'tp'), may hold values from 0.001 to 0.02
- key_first: float32 [128, 1024], P(None, 'tp'), may hold values from -0.75 to 0.75
- key_second: float32 [128, 1024], P(None, 'tp'), may hold values from 0.001 to 0.02
- branch_first: float32 [4096, 128], P('fs'), may hold values from -0.75 to 0.75
- branch_second: float32 [4096, 128], P('fs'), may hold values from 0.001 to 0.02
Outputs:
- query_step: float32 [4096, 4096], P('fs', 'tp')
- key_step: float32 [4096, 1024], P('fs', 'tp')
- branch_step: float32 [4096, 4096], P('fs', 'tp')
- query_updated: float32 [4096, 4096], P('fs', 'tp')
- key_updated: float32 [4096, 1024], P('fs', 'tp')
- branch_updated: float32 [4096, 4096], P('fs', 'tp')
- query_copy: bfloat16 [4096, 4096], P(None, 'tp')
- key_copy: bfloat16 [4096, 1024], P(None, 'tp')
- branch_copy: bfloat16 [4096, 4096], P(None, 'tp')
- query_first_new: float32 [128, 4096], P(None, 'tp')
- query_second_new: float32 [128, 4096], P(None, 'tp')
- key_first_new: float32 [128, 1024], P(None, 'tp')
- key_second_new: float32 [128, 1024], P(None, 'tp')
- branch_first_new: float32 [4096, 128], P('fs')
- branch_second_new: float32 [4096, 128], P('fs')
All inputs are finite; a program needn't handle non-finite values.
Results may differ from a plain program's by a relative error of at most 0.001.
Values may be sent and summed in bfloat16 or wider, within the bound.
A program may use at most 128 MiB of HBM per device.

v0:
```python
import functools

import jax
import jax.numpy as jnp
from jax import lax
from jax.experimental import pallas as pl
from jax.experimental.pallas import tpu as pltpu
from jax.sharding import PartitionSpec as P

LEARN = 0.02
BETA_ONE = 0.9
BETA_TWO = 0.95
ADAM_EPS = 1e-08
CLIP_RMS = 0.5


def moments(first, second, low, clip):
    scaled = clip * low
    first_new = BETA_ONE * first + (1.0 - BETA_ONE) * scaled
    second_new = BETA_TWO * second + (1.0 - BETA_TWO) * scaled * scaled
    return (first_new, second_new, first_new / (jnp.sqrt(second_new) + ADAM_EPS))


def over_tokens(left, right, precision=None):
    return lax.dot_general(
        left,
        right,
        (((0,), (0,)), ((), ())),
        precision=precision,
        preferred_element_type=jnp.float32,
    )


def split_three(values):
    high = values.astype(jnp.bfloat16)
    rest = values - high.astype(jnp.float32)
    middle = rest.astype(jnp.bfloat16)
    low = (rest - middle.astype(jnp.float32)).astype(jnp.bfloat16)
    return high, middle, low


class Sender:
    def __init__(self, send_sem, recv_sem):
        self.send_sem, self.recv_sem, self.used, self.started = send_sem, recv_sem, 0, []

    def start(self, source, target, device):
        copy = pltpu.make_async_remote_copy(
            src_ref=source,
            dst_ref=target,
            send_sem=self.send_sem.at[self.used],
            recv_sem=self.recv_sem.at[self.used],
            device_id=device,
            device_id_type=pl.DeviceIdType.MESH,
        )
        self.used += 1
        copy.start()
        self.started.append(copy)
        return copy

    def drain(self):
        for copy in self.started:
            copy.wait_send()


def greet(nf, nt, row, col, both):
    barrier = pltpu.get_barrier_semaphore()
    peers = [{"fs": lax.rem(row + o, nf), "tp": col} for o in range(1, nf)]
    if both:
        peers += [{"fs": row, "tp": lax.rem(col + o, nt)} for o in range(1, nt)]
    for peer in peers:
        pl.semaphore_signal(
            barrier, inc=1, device_id=peer, device_id_type=pl.DeviceIdType.MESH
        )
    pl.semaphore_wait(barrier, len(peers))


def square(row, col):
    side = row + 1 - 2 * lax.rem(row, 2)
    front = lax.rem(row + 2, 4)
    return side, front, ({"fs": side, "tp": col}, {"fs": front, "tp": col})


def reduce_kernel(
    nf, nt,
    x_hbm, qu_hbm, ku_hbm, h_hbm, bu_hbm, master_ref, qb_ref, kb_ref, bb_ref,
    qk_out, b_out, total_out, far_out,
    x_ref, qu_ref, ku_ref, h_ref, bu_ref,
    part, from_pair, halves, arrived, whole, other,
    part_qk, part_b, got_qk, got_b, all_qk, all_b, spread_b, sums,
    send_sem, recv_sem, load_sem,
):
    row, col = lax.axis_index("fs"), lax.axis_index("tp")
    core, height = lax.rem(col, 2), lax.div(col, 2)
    nz = nt // 2
    rank = qb_ref.shape[1]
    half = x_ref.shape[0] // 2
    piece = half // nz
    query_cols = qu_ref.shape[1]
    loads = []

    def load(source, target):
        copy = pltpu.make_async_copy(source, target, load_sem.at[len(loads)])
        copy.start()
        loads.append(copy)

    for which in (1 - core, core):
        rows = pl.ds(pl.multiple_of(which * half, half), half)
        load(x_hbm.at[rows], x_ref.at[rows])
        load(bu_hbm.at[rows], bu_ref.at[rows])
    load(qu_hbm, qu_ref)
    load(ku_hbm, ku_ref)
    load(h_hbm, h_ref)
    greet(nf, nt, row, col, True)
    sender = Sender(send_sem, recv_sem)
    pair = {"fs": row, "tp": height * 2 + (1 - core)}

    def above(o):
        return {"fs": row, "tp": lax.rem(height + o, nz) * 2 + core}

    def beside(o):
        return {"fs": lax.rem(row + o, nf), "tp": col}

    def project(which):
        rows = pl.ds(pl.multiple_of(which * half, half), half)
        x = x_ref[rows, :]
        return (
            jnp.dot(x, qb_ref[...], preferred_element_type=jnp.float32),
            jnp.dot(x, kb_ref[...], preferred_element_type=jnp.float32),
            jnp.dot(bu_ref[rows, :], bb_ref[...], preferred_element_type=jnp.float32),
        )

    early = far_out.shape[1]
    sent = []
    if nf == 4:
        side, front, names = square(row, col)
        for turn in range(2):
            for n in range(2):
                rows = pl.ds((turn ^ n) * (early // 2), early // 2)
                sent.append(
                    sender.start(master_ref.at[rows], far_out.at[row, rows], names[n])
                )
    else:
        rows = pl.ds(0, early)
        for o in range(1, nf):
            sent.append(sender.start(master_ref.at[rows], far_out.at[row], beside(o)))
    loads[0].wait()
    loads[1].wait()
    for n, value in enumerate(project(1 - core)):
        part[:, n * rank : (n + 1) * rank] = value
    swap = sender.start(part, from_pair, pair)
    loads[2].wait()
    loads[3].wait()
    own = project(core)
    swap.wait_recv()
    for n, value in enumerate(own):
        span = slice(n * rank, (n + 1) * rank)
        halves[:, :, span] = (value + from_pair[:, span]).reshape(nz, piece, rank)
    copies = [
        sender.start(halves.at[lax.rem(height + o, nz)], arrived.at[o - 1], above(o))
        for o in range(1, nz)
    ]
    total = halves[height]
    for o, copy in enumerate(copies):
        copy.wait_recv()
        total = total + arrived[o]
    whole[height] = total
    copies = [sender.start(whole.at[height], whole.at[height], above(o)) for o in range(1, nz)]
    across = [sender.start(whole.at[height], other.at[height], pair)]
    passed = []
    if nf == 4:
        for n, source in ((0, side), (1, front)):
            sent[n].wait_recv()
            held = far_out.at[source, pl.ds(n * (early // 2), early // 2)]
            passed.append(sender.start(held, held, names[1 - n]))
    for o, copy in enumerate(copies, 1):
        copy.wait_recv()
        source = lax.rem(height + nz - o, nz)
        across.append(sender.start(whole.at[source], other.at[source], pair))

    over_rows = (((0,), (0,)), ((), ()))

    def low_parts(values, which):
        rows = pl.ds(pl.multiple_of(which * half, half), half)
        sides = (qu_ref[rows, :], ku_ref[rows, :], h_ref[rows, :])
        parts = []
        for n, side in enumerate(sides):
            terms = split_three(values[:, n * rank : (n + 1) * rank])
            parts.append(
                sum(
                    lax.dot_general(term, side, over_rows, preferred_element_type=jnp.float32)
                    for term in terms
                )
            )
        return parts

    for copy in loads[4:]:
        copy.wait()
    first = low_parts(whole[...].reshape(half, 3 * rank), core)
    for copy in across:
        copy.wait_recv()
    second = low_parts(other[...].reshape(half, 3 * rank), 1 - core)
    query_part, key_part, branch_part = [a + b for a, b in zip(first, second)]
    part_qk[:, :, :query_cols] = query_part.reshape(nf, rank // nf, query_cols)
    part_qk[:, :, query_cols:] = key_part.reshape(nf, rank // nf, key_part.shape[1])
    part_b[...] = branch_part.T.reshape(part_b.shape)

    copies = []
    for o in range(1, nf):
        to = lax.rem(row + o, nf)
        copies.append(sender.start(part_qk.at[to], got_qk.at[o - 1], beside(o)))
        copies.append(sender.start(part_b.at[to], got_b.at[o - 1], beside(o)))
    for copy in copies:
        copy.wait_recv()
    sum_qk, sum_b = part_qk[row], part_b[row]
    for o in range(nf - 1):
        sum_qk = sum_qk + got_qk[o]
        sum_b = sum_b + got_b[o]
    rows_b = sum_b.shape[0]
    squares = jnp.sum(sum_qk * sum_qk) + jnp.sum(sum_b * sum_b)
    all_qk[row] = sum_qk
    all_b[col, :rows_b, :] = sum_b
    all_b[col, rows_b:, :] = jnp.full((8, rank), squares, jnp.float32)

    copies_b = [
        sender.start(all_b.at[col], all_b.at[col], {"fs": row, "tp": lax.rem(col + o, nt)})
        for o in range(1, nt)
    ]
    copies_qk = [sender.start(all_qk.at[row], all_qk.at[row], beside(o)) for o in range(1, nf)]
    for copy in copies_b:
        copy.wait_recv()
    sums[row] = jnp.sum(all_b[:, rows_b:, :], axis=0)
    each = nt // nf
    copies = []
    for o in range(1, nf):
        blocks = pl.ds(lax.rem(row + o, nf) * each, each)
        copies.append(sender.start(sums.at[row], sums.at[row], beside(o)))
        copies.append(sender.start(all_b.at[blocks], spread_b.at[row], beside(o)))
    b_out[:, row] = all_b[pl.ds(row * each, each)][:, :rows_b, :]
    for copy in copies_qk:
        copy.wait_recv()
    qk_out[...] = all_qk[...].reshape(qk_out.shape)
    for copy in copies:
        copy.wait_recv()
    for o in range(1, nf):
        source = lax.rem(row + o, nf)
        b_out[:, source] = spread_b[source][:, :rows_b, :]
    total_out[...] = jnp.sum(sums[...], axis=0)
    for copy in (sent[2:] + passed) if nf == 4 else sent:
        copy.wait_recv()
    sender.drain()


def reduced(nf, nt, early, x, qu, ku, h, bu, master, qb, kb, bb):
    tokens, features = x.shape
    rank = qb.shape[1]
    cols = qu.shape[1] + ku.shape[1]
    half, nz, each = tokens // 2, nt // 2, nt // nf
    piece, thin, rows_b = half // nz, rank // nf, features // nf
    copies = 1 + 2 * (nz - 1) + nz + 2 * (nf - 1) + (nt - 1) + 3 * (nf - 1)
    copies += 6 if nf == 4 else nf - 1
    any_place = pl.BlockSpec(memory_space=pl.ANY)
    vmem = pl.BlockSpec(memory_space=pltpu.VMEM)
    f32 = jnp.float32
    return pl.pallas_call(
        functools.partial(reduce_kernel, nf, nt),
        out_shape=(
            jax.ShapeDtypeStruct((rank, cols), f32),
            jax.ShapeDtypeStruct((each, nf, rows_b, rank), f32),
            jax.ShapeDtypeStruct((8, rank), f32),
            jax.ShapeDtypeStruct((nf, early, master.shape[1]), f32),
        ),
        in_specs=[any_place] * 6 + [vmem] * 3,
        out_specs=(vmem, vmem, vmem, any_place),
        scratch_shapes=[
            *[pltpu.VMEM(each_in.shape, each_in.dtype) for each_in in (x, qu, ku, h, bu)],
            pltpu.VMEM((half, 3 * rank), f32),
            pltpu.VMEM((half, 3 * rank), f32),
            pltpu.VMEM((nz, piece, 3 * rank), f32),
            pltpu.VMEM((nz - 1, piece, 3 * rank), f32),
            pltpu.VMEM((nz, piece, 3 * rank), f32),
            pltpu.VMEM((nz, piece, 3 * rank), f32),
            pltpu.VMEM((nf, thin, cols), f32),
            pltpu.VMEM((nf, rows_b, rank), f32),
            pltpu.VMEM((nf - 1, thin, cols), f32),
            pltpu.VMEM((nf - 1, rows_b, rank), f32),
            pltpu.VMEM((nf, thin, cols), f32),
            pltpu.VMEM((nt, rows_b + 8, rank), f32),
            pltpu.VMEM((nf, each, rows_b + 8, rank), f32),
            pltpu.VMEM((nf, 8, rank), f32),
            pltpu.SemaphoreType.DMA((copies,)),
            pltpu.SemaphoreType.DMA((copies,)),
            pltpu.SemaphoreType.DMA((7,)),
        ],
        compiler_params=pltpu.CompilerParams(
            collective_id=0, has_side_effects=True, vmem_limit_bytes=58 * 2**20
        ),
    )(x, qu, ku, h, bu, master, qb, kb, bb)


def gather_kernel(
    nf, nt,
    q_ref, b_ref, k_ref, far_ref, master_ref, basis_ref, dir_ref,
    q_out, b_out, k_out,
    held_far, held_copy, send_sem, recv_sem, own_sem, load_sem, store_sem,
):
    row, col = lax.axis_index("fs"), lax.axis_index("tp")
    early = far_ref.shape[1]
    pairs = ((q_ref, q_out, early), (b_ref, b_out, 0), (k_ref, k_out, 0))

    def load(o):
        source = master_ref.at[pl.ds(0, early)] if o == 0 else far_ref.at[lax.rem(row + o, nf)]
        copy = pltpu.make_async_copy(source, held_far.at[o % 2], load_sem.at[o])
        copy.start()
        return copy

    coming = load(0)
    greet(nf, nt, row, col, False)
    sender = Sender(send_sem, recv_sem)
    sent = []
    if nf == 4:
        side, front, names = square(row, col)
        for ref, out, base in pairs:
            half = ref.shape[0] // 2
            for h in range(2):
                rows = pl.ds(h * half, half)
                target = pl.ds(base + h * half, half)
                for n in ((0, 1), (1, 0))[h]:
                    copy = sender.start(ref.at[rows], out.at[row, target], names[n])
                    sent.append((n, h, out, target, copy))
    else:
        for ref, out, base in pairs:
            for o in range(1, nf):
                target = out.at[row, pl.ds(base, ref.shape[0])]
                there = {"fs": lax.rem(row + o, nf), "tp": col}
                sent.append(sender.start(ref, target, there))
    local = []
    for n, (ref, out, base) in enumerate(pairs):
        target = out.at[row, pl.ds(base, ref.shape[0])]
        local.append(pltpu.make_async_copy(ref, target, own_sem.at[n]))
        local[-1].start()

    terms = split_three(dir_ref[...])
    rows_all = q_out.shape[1]
    stores = []
    for o in range(nf):
        source = lax.rem(row + o, nf)
        coming.wait()
        if o + 1 < nf:
            coming = load(o + 1)
        if o >= 2:
            stores[o - 2].wait()
        basis = basis_ref[pl.ds(pl.multiple_of(source * rows_all, rows_all), early), :]
        step = sum(jnp.dot(basis, term, preferred_element_type=jnp.float32) for term in terms)
        held_copy[o % 2] = (held_far[o % 2] - LEARN * step).astype(held_copy.dtype)
        stores.append(
            pltpu.make_async_copy(
                held_copy.at[o % 2], q_out.at[source, pl.ds(0, early)], store_sem.at[o]
            )
        )
        stores[-1].start()

    if nf == 4:
        last = []
        for n, h, out, target, copy in sent:
            copy.wait_recv()
            if n == h:
                held = out.at[(side, front)[n], target]
                last.append(sender.start(held, held, names[1 - n]))
        sent = last
    for copy in sent:
        copy.wait_recv()
    for copy in local + stores[-2:]:
        copy.wait()
    sender.drain()


def gathered_rows(nf, nt, q_tail, b_block, k_block, far, master, basis, direction):
    count = 18 if nf == 4 else 3 * (nf - 1)
    early = far.shape[1]
    blocks = (master, b_block, k_block)
    wide = [jax.ShapeDtypeStruct((nf, *block.shape), q_tail.dtype) for block in blocks]
    vmem = pl.BlockSpec(memory_space=pltpu.VMEM)
    any_place = pl.BlockSpec(memory_space=pl.ANY)
    outs = pl.pallas_call(
        functools.partial(gather_kernel, nf, nt),
        out_shape=tuple(wide),
        in_specs=[vmem] * 3 + [any_place] * 2 + [vmem] * 2,
        out_specs=(any_place,) * 3,
        scratch_shapes=[
            pltpu.VMEM((2, early, far.shape[2]), far.dtype),
            pltpu.VMEM((2, early, far.shape[2]), q_tail.dtype),
            pltpu.SemaphoreType.DMA((count,)),
            pltpu.SemaphoreType.DMA((count,)),
            pltpu.SemaphoreType.DMA((3,)),
            pltpu.SemaphoreType.DMA((nf,)),
            pltpu.SemaphoreType.DMA((nf,)),
        ],
        compiler_params=pltpu.CompilerParams(
            collective_id=1, has_side_effects=True, vmem_limit_bytes=48 * 2**20
        ),
    )(q_tail, b_block, k_block, far, master, basis, direction)
    return [out.reshape(-1, out.shape[-1]) for out in outs]


def per_device(
    normed_inputs,
    query_upstream,
    key_upstream,
    head_outputs,
    branch_upstream,
    query_master,
    key_master,
    branch_master,
    query_basis,
    key_basis,
    branch_basis,
    query_first,
    query_second,
    key_first,
    key_second,
    branch_first,
    branch_second,
):
    exact = lax.Precision.HIGHEST
    row_index = lax.axis_index("fs")
    col_index = lax.axis_index("tp")
    n_rows = lax.axis_size("fs")
    n_cols = lax.axis_size("tp")
    features = normed_inputs.shape[1]
    query_local = query_upstream.shape[1]
    key_local = key_upstream.shape[1]
    rows_in = query_master.shape[0]
    rank = query_basis.shape[1]
    def own_block(basis):
        return lax.dynamic_slice_in_dim(basis, col_index * features, features, 0)

    block_branch = own_block(branch_basis)
    own_branch = block_branch.astype(jnp.float32)
    lanes = -key_local % 128
    early = rows_in // 32 * 20
    low, branch_low, squares, far = reduced(
        n_rows,
        n_cols,
        early,
        normed_inputs,
        query_upstream,
        jnp.pad(key_upstream, ((0, 0), (0, lanes))),
        head_outputs,
        branch_upstream,
        query_master,
        own_block(query_basis),
        own_block(key_basis),
        block_branch,
    )
    query_low = low[:, :query_local]
    key_low = low[:, query_local : query_local + key_local]
    branch_low = branch_low.reshape(branch_first.shape)
    total = squares[0, 0]
    entries = rank * n_cols * (2 * query_local + key_local)
    rms_value = jnp.sqrt(total / float(entries))
    clip = 1.0 / jnp.maximum(1.0, rms_value / CLIP_RMS)
    q_first, q_second, q_dir = moments(query_first, query_second, query_low, clip)
    k_first, k_second, k_dir = moments(key_first, key_second, key_low, clip)
    b_first, b_second, b_dir = moments(branch_first, branch_second, branch_low, clip)
    step_rows_query = lax.dynamic_slice_in_dim(query_basis, row_index * rows_in, rows_in, 0).astype(
        jnp.float32
    )
    step_rows_key = lax.dynamic_slice_in_dim(key_basis, row_index * rows_in, rows_in, 0).astype(
        jnp.float32
    )
    query_step = jnp.dot(step_rows_query, q_dir, precision=exact)
    key_step = jnp.dot(step_rows_key, k_dir, precision=exact)
    branch_step = jnp.dot(b_dir, own_branch.T, precision=exact)
    query_updated = query_master - LEARN * query_step
    key_updated = key_master - LEARN * key_step
    branch_updated = branch_master - LEARN * branch_step
    query_copy, branch_copy, key_copy = gathered_rows(
        n_rows,
        n_cols,
        query_updated[early:].astype(jnp.bfloat16),
        branch_updated.astype(jnp.bfloat16),
        jnp.pad(key_updated, ((0, 0), (0, lanes))).astype(jnp.bfloat16),
        far,
        query_master,
        query_basis,
        q_dir,
    )
    key_copy = key_copy[:, :key_local]
    return (
        query_step,
        key_step,
        branch_step,
        query_updated,
        key_updated,
        branch_updated,
        query_copy,
        key_copy,
        branch_copy,
        q_first,
        q_second,
        k_first,
        k_second,
        b_first,
        b_second,
    )


def solution(mesh):
    return jax.shard_map(
        per_device,
        mesh=mesh,
        in_specs=(
            P("fs", "tp"),
            P("fs", "tp"),
            P("fs", "tp"),
            P("fs", "tp"),
            P("fs", "tp"),
            P("fs", "tp"),
            P("fs", "tp"),
            P("fs", "tp"),
            P(),
            P(),
            P(),
            P(None, "tp"),
            P(None, "tp"),
            P(None, "tp"),
            P(None, "tp"),
            P("fs", None),
            P("fs", None),
        ),
        out_specs=(
            P("fs", "tp"),
            P("fs", "tp"),
            P("fs", "tp"),
            P("fs", "tp"),
            P("fs", "tp"),
            P("fs", "tp"),
            P(None, "tp"),
            P(None, "tp"),
            P(None, "tp"),
            P(None, "tp"),
            P(None, "tp"),
            P(None, "tp"),
            P(None, "tp"),
            P("fs", None),
            P("fs", None),
        ),
        check_vma=False,
    )
```

profile of v0, /device:TPU:27, one launch (start us, length us, event | category | flops | bytes accessed | tf_op | source)
XLA Modules:
  0.0 161.4 jit_solution(16009368587692755878)
XLA Ops:
  0.7 1.6 constant_dynamic-slice_fusion.2.qb_ref
  2.2 1.7 %constant_dynamic-slice_fusion = (bf16[512,128]{1,0:T(8,128)(2,1)}, bf16[512,128]{1,0:T(8,128)(2,1)}) fusion(bf16[4096,128]{1,0:T(8,128)(2,1)} %param.27, s32[]{:T(128)S(6)} %select_n.10, bf16[4096,128]{1,0:T(8,128)(2,1)} %param.26), kind=kLoop, calls=%fused_computation.32 | loop fusion | bytes 524292 | tf_op jit(solution)/shard_map/dynamic_slice | solution.py:435
  3.9 77.9 %shard_map.280 = (f32[128,640]{1,0:T(8,128)}, f32[2,4,128,128]{3,2,1,0:T(8,128)}, f32[8,128]{1,0:T(8,128)}, f32[4,640,512]{2,1,0:T(8,128)}) custom-call(bf16[1024,512]{1,0:T(8,128)(2,1)} %x_hbm.1, bf16[1024,512]{1,0:T(8,128)(2,1)} %qu_hbm.1, bf16[1024,128]{1,0:T(8,128)(2,1)} %ku_hbm.1, bf16[1024,512]{1,0:T(8,128)(2,1)} %h_hbm.1, bf16[1024,512]{1,0:T(8,128)(2,1)} %bu_hbm.1, ...), custom_call_target="tpu_custom_call" | custom-call | tf_op jit(solution)/shard_map/pallas_call | solution.py:264
  81.9 0.0 copy-start.8
  81.9 0.0 copy-start.9
  81.9 1.3 slice.13
  83.9 1.1 broadcast_multiply_fusion
  85.0 0.9 fusion.12
  85.9 0.0 copy-start.11
  85.9 0.0 copy-start.12
  85.9 0.0 copy-start.10
  85.9 2.0 %add_divide_fusion = (f32[128,512]{1,0:T(8,128)S(1)}, f32[128,512]{1,0:T(8,128)}, f32[128,512]{1,0:T(8,128)}) fusion(f32[128,640]{1,0:T(8,128)} %get-tuple-element.23, f32[]{:T(128)} %bitcast, f32[128,512]{1,0:T(8,128)S(1)} %copy-done.13, f32[128,512]{1,0:T(8,128)S(1)} %copy-done.14), kind=kLoop, calls=%fused_computation.18 | loop fusion | flops 655360 | bytes 1572868 | tf_op jit(solution)/shard_map/div | solution.py:21
  87.9 0.0 copy-start.1
  87.9 0.2 fusion
  88.1 0.0 copy-start.4
  88.1 0.0 copy-start.5
  88.1 2.8 %fusion.21 = (bf16[1024,128]{1,0:T(8,128)(2,1)S(1)}, f32[1024,128]{1,0:T(8,128)}, f32[1024,128]{1,0:T(8,128)}) fusion(f32[1024,128]{1,0:T(8,128)S(1)} %copy-done.10, f32[128,128]{1,0:T(8,128)S(1)} %get-tuple-element.72, f32[128,128]{1,0:T(8,128)S(1)} %get-tuple-element.73, bf16[4096,128]{1,0:T(8,128)(2,1)} %param.26, s32[]{:T(128)S(6)} %select_n.4), kind=kOutput, calls=%fused_computation.38 | convolution fusion | flops 201752576 | bytes 2228228 | tf_op jit(solution)/shard_map/dot_general | solution.py:472
  90.9 0.0 copy-start.7
  91.0 2.4 %multiply_subtract_fusion.1 = (f32[1024,512]{1,0:T(8,128)S(1)}, f32[1024,512]{1,0:T(8,128)}) fusion(f32[1024,512]{1,0:T(8,128)S(1)} %copy-done, f32[128,512]{1,0:T(8,128)S(1)} %get-tuple-element.33.dir_ref, bf16[4096,128]{1,0:T(8,128)(2,1)S(1)} %copy-done.1, s32[]{:T(128)S(6)} %select_n.4), kind=kOutput, calls=%fused_computation.1 | convolution fusion | flops 806354944 | bytes 6815748 | tf_op jit(solution)/shard_map/dot_general | solution.py:471
  93.5 3.2 %fusion.22 = (bf16[1024,512]{1,0:T(8,128)(2,1)S(1)}, f32[1024,512]{1,0:T(8,128)}, f32[1024,512]{1,0:T(8,128)}) fusion(f32[1024,512]{1,0:T(8,128)S(1)} %copy-done.6, bf16[512,128]{1,0:T(8,128)(2,1)S(1)} %copy-done.7, f32[1024,128]{1,0:T(8,128)S(1)} %get-tuple-element.74, f32[1024,128]{1,0:T(8,128)S(1)} %get-tuple-element.75), kind=kOutput, calls=%fused_computation.39 | convolution fusion | flops 807141376 | bytes 8519680 | tf_op jit(solution)/shard_map/dot_general | solution.py:473
  96.7 57.1 %shard_map.281 = (bf16[4,1024,512]{2,1,0:T(8,128)(2,1)}, bf16[4,1024,512]{2,1,0:T(8,128)(2,1)}, bf16[4,1024,128]{2,1,0:T(8,128)(2,1)S(1)}) custom-call(bf16[384,512]{1,0:T(8,128)(2,1)S(1)} %slice.29.q_ref, bf16[1024,512]{1,0:T(8,128)(2,1)S(1)} %get-tuple-element.31.b_ref, bf16[1024,128]{1,0:T(8,128)(2,1)S(1)} %get-tuple-element.29.k_ref, ...), custom_call_target="tpu_custom_call" | custom-call | tf_op jit(solution)/shard_map/pallas_call | solution.py:384
  153.7 4.6 %copy.35 = bf16[4096,512]{1,0:T(8,128)(2,1)} copy(bf16[4096,512]{1,0:T(8,128)(2,1)} %bitcast.13) | data formatting | bytes 8388608
  158.4 1.0 copy.36
  159.3 2.0 %copy.37 = bf16[4096,512]{1,0:T(8,128)(2,1)} copy(bf16[4096,512]{1,0:T(8,128)(2,1)S(1)} %bitcast.12) | data formatting | bytes 8388608
  (26 shorter events, 0.1 us)
Async XLA Ops:
  3.9 81.1 %copy-start.15 = (f32[128,128]{1,0:T(8,128)S(1)}, f32[128,128]{1,0:T(8,128)}, u32[]{:S(2)}) copy-start(f32[128,128]{1,0:T(8,128)} %param.31) | copy-start | bytes 196612
  3.9 81.1 %copy-start.16 = (f32[128,128]{1,0:T(8,128)S(1)}, f32[128,128]{1,0:T(8,128)}, u32[]{:S(2)}) copy-start(f32[128,128]{1,0:T(8,128)} %param.30) | copy-start | bytes 196612
  3.9 82.0 %copy-start.13 = (f32[128,512]{1,0:T(8,128)S(1)}, f32[128,512]{1,0:T(8,128)}, u32[]{:S(2)}) copy-start(f32[128,512]{1,0:T(8,128)} %param.29) | copy-start | bytes 786436
  3.9 82.0 %copy-start.14 = (f32[128,512]{1,0:T(8,128)S(1)}, f32[128,512]{1,0:T(8,128)}, u32[]{:S(2)}) copy-start(f32[128,512]{1,0:T(8,128)} %param.28) | copy-start | bytes 786436
  81.9 6.0 %copy-start.8 = (f32[1024,128]{1,0:T(8,128)S(1)}, f32[1024,128]{1,0:T(8,128)}, u32[]{:S(2)}) copy-start(f32[1024,128]{1,0:T(8,128)} %param.33) | copy-start | bytes 1572868
  81.9 6.0 %copy-start.9 = (f32[1024,128]{1,0:T(8,128)S(1)}, f32[1024,128]{1,0:T(8,128)}, u32[]{:S(2)}) copy-start(f32[1024,128]{1,0:T(8,128)} %param.32) | copy-start | bytes 1572868
  85.9 2.2 %copy-start.11 = (f32[128,128]{1,0:T(8,128)}, f32[128,128]{1,0:T(8,128)S(1)}, u32[]{:S(2)}) copy-start(f32[128,128]{1,0:T(8,128)S(1)} %get-tuple-element.73) | copy-start | bytes 196612
  85.9 2.2 %copy-start.12 = (f32[128,128]{1,0:T(8,128)}, f32[128,128]{1,0:T(8,128)S(1)}, u32[]{:S(2)}) copy-start(f32[128,128]{1,0:T(8,128)S(1)} %get-tuple-element.72) | copy-start | bytes 196612
  85.9 2.2 %copy-start.10 = (f32[1024,128]{1,0:T(8,128)S(1)}, f32[1024,128]{1,0:T(8,128)}, u32[]{:S(2)}) copy-start(f32[1024,128]{1,0:T(8,128)} %param.23) | copy-start | bytes 1572868
  87.9 3.1 %copy-start = (f32[1024,512]{1,0:T(8,128)S(1)}, f32[1024,512]{1,0:T(8,128)}, u32[]{:S(2)}) copy-start(f32[1024,512]{1,0:T(8,128)} %master_ref.3) | copy-start | bytes 6291460
  87.9 3.1 %copy-start.1 = (bf16[4096,128]{1,0:T(8,128)(2,1)S(1)}, bf16[4096,128]{1,0:T(8,128)(2,1)}, u32[]{:S(2)}) copy-start(bf16[4096,128]{1,0:T(8,128)(2,1)} %basis_ref.1) | copy-start | bytes 3145732
  88.1 5.4 %copy-start.4 = (f32[1024,128]{1,0:T(8,128)}, f32[1024,128]{1,0:T(8,128)S(1)}, u32[]{:S(2)}) copy-start(f32[1024,128]{1,0:T(8,128)S(1)} %get-tuple-element.75) | copy-start | bytes 1572868
  88.1 5.4 %copy-start.5 = (f32[1024,128]{1,0:T(8,128)}, f32[1024,128]{1,0:T(8,128)S(1)}, u32[]{:S(2)}) copy-start(f32[1024,128]{1,0:T(8,128)S(1)} %get-tuple-element.74) | copy-start | bytes 1572868
  90.9 2.5 %copy-start.6 = (f32[1024,512]{1,0:T(8,128)S(1)}, f32[1024,512]{1,0:T(8,128)}, u32[]{:S(2)}) copy-start(f32[1024,512]{1,0:T(8,128)} %param.24) | copy-start | bytes 6291460
  90.9 2.5 %copy-start.7 = (bf16[512,128]{1,0:T(8,128)(2,1)S(1)}, bf16[512,128]{1,0:T(8,128)(2,1)}, u32[]{:S(2)}) copy-start(bf16[512,128]{1,0:T(8,128)(2,1)} %get-tuple-element.44.bb_ref) | copy-start | bytes 393220
  93.4 3.3 %copy-start.3 = (f32[1024,512]{1,0:T(8,128)}, f32[1024,512]{1,0:T(8,128)S(1)}, u32[]{:S(2)}) copy-start(f32[1024,512]{1,0:T(8,128)S(1)} %get-tuple-element.64) | copy-start | bytes 6291460
  153.7 5.6 %copy-start.2 = (bf16[4,1024,512]{2,1,0:T(8,128)(2,1)S(1)}, bf16[4,1024,512]{2,1,0:T(8,128)(2,1)}, u32[]{:S(2)}) copy-start(bf16[4,1024,512]{2,1,0:T(8,128)(2,1)} %get-tuple-element.28) | copy-start | bytes 12582916
where the time goes:
time: 164 us; the launch traced here: 161 us
  Pallas kernels  135 us (82%)
  local copies, waits for them, and re-layouts  12.3 us (8%)
  matrix products  8.42 us (5%)
  other arithmetic  4.05 us (2%)
    pallas_call x1, Pallas kernels, reduced(): pl.pallas_call(functools.partial(reduce_kernel, nf, nt), out_shape=(jax.S...  77.9 us
    pallas_call x1, Pallas kernels, gathered_rows(): pl.pallas_call(functools.partial(gather_kernel, nf, nt), out_shape=tuple(...  57.1 us
    unnamed x37, local copies, waits for them, and re-layouts  7.71 us

commit v1 on v0

--- a/solution.py
+++ b/solution.py
@@ -42,6 +42,10 @@
 class Sender:
     def __init__(self, send_sem, recv_sem):
         self.send_sem, self.recv_sem, self.used, self.started = send_sem, recv_sem, 0, []
+
+    def reserve(self, count):
+        self.used += count
+        return self.used - count
 
     def start(self, source, target, device):
         copy = pltpu.make_async_remote_copy(
@@ -402,6 +406,447 @@
     return [out.reshape(-1, out.shape[-1]) for out in outs]
 
 
+EARLY_OF_64 = 56
+VMEM_LIMIT = 40 * 2**20
+MASTER_MOST = 0.09375
+MASTER_POWER = 14
+MASTER_GAIN = 515.0 / MASTER_MOST
+SUM_POWER = 16
+SUM_GAIN = 238.0
+
+
+def raised(magnitude, power):
+    result, square = None, magnitude
+    while power:
+        if power % 2:
+            result = square if result is None else result * square
+        power //= 2
+        if power:
+            square = square * square
+    return result
+
+
+def coded(values, power):
+    high = raised(jnp.abs(values), power)
+    return jnp.where(values < 0, -high, high).astype(jnp.bfloat16)
+
+
+def decoded(codes, power):
+    codes = codes.astype(jnp.float32)
+    root = jnp.exp(jnp.log(jnp.abs(codes)) * (1.0 / power))
+    root = jnp.where(codes == 0, 0.0, root)
+    return jnp.where(codes < 0, -root, root)
+
+
+def column_scale(values):
+    most = jnp.max(jnp.abs(values), axis=0, keepdims=True)
+    return jnp.maximum(most, 1e-30).astype(jnp.bfloat16)
+
+
+def pack_columns(values):
+    scale = column_scale(values)
+    codes = coded(values * (SUM_GAIN / scale.astype(jnp.float32)), SUM_POWER)
+    return codes, jnp.broadcast_to(scale, (16, values.shape[1]))
+
+
+def unpack_columns(codes, scale):
+    return decoded(codes, SUM_POWER) * (scale[0:1].astype(jnp.float32) * (1.0 / SUM_GAIN))
+
+
+def split_two(values):
+    high = values.astype(jnp.bfloat16)
+    return high, (values - high.astype(jnp.float32)).astype(jnp.bfloat16)
+
+
+def exact_dot(left, terms):
+    return sum(jnp.dot(left, term, preferred_element_type=jnp.float32) for term in terms)
+
+
+def fused_kernel(
+    nf, nt, early,
+    x_hbm, qu_hbm, ku_hbm, h_hbm, bu_hbm, mq_hbm, mk_hbm, mb_hbm, qb_hbm, kb_hbm, bb_hbm,
+    qf_hbm, qs_hbm, kf_hbm, ks_hbm, bf_hbm, bs_hbm,
+    q_step, k_step, b_step, q_new, k_new, b_new, q_out, k_out, b_out,
+    qf_out, qs_out, kf_out, ks_out, bf_out, bs_out,
+    x_ref, qu_ref, ku_ref, h_ref, bu_ref, mq_ref, mk_ref, mb_ref, qb_ref, kb_ref,
+    qf_ref, qs_ref, kf_ref, ks_ref, bf_ref, bs_ref, own_ref, turned, bbt_ref,
+    part, from_pair, halves, sent_z, arrived, whole, other, split_ref,
+    part_qk, part_b, got_qk, got_b, all_qk, own_b, blocks_b, pair_b, sums_f, sums_t,
+    enc, far,
+    send_sem, recv_sem, load_sem, b_recv,
+):
+    row, col = lax.axis_index("fs"), lax.axis_index("tp")
+    core, height = lax.rem(col, 2), lax.div(col, 2)
+    nz = nt // 2
+    rank = qb_ref.shape[1]
+    tokens, features = x_ref.shape
+    half = tokens // 2
+    piece = half // nz
+    query_cols, key_cols = qu_ref.shape[1], ku_ref.shape[1]
+    rows_in = mq_ref.shape[0]
+    loads = {}
+
+    def load(name, source, target):
+        copy = pltpu.make_async_copy(source, target, load_sem.at[len(loads)])
+        copy.start()
+        loads[name] = copy
+
+    def token_rows(which):
+        return pl.ds(pl.multiple_of(which * half, half), half)
+
+    first, second = pl.ds(0, early // 2), pl.ds(early // 2, early // 2)
+    load("mq0", mq_hbm.at[first], mq_ref.at[first])
+    load("mq1", mq_hbm.at[second], mq_ref.at[second])
+    own_rows = pl.ds(pl.multiple_of(col * features, features), features)
+    for n, basis in enumerate((qb_hbm, kb_hbm, bb_hbm)):
+        load(("own", n), basis.at[own_rows], own_ref.at[n])
+    for n, which in enumerate((1 - core, core)):
+        load(("x", n), x_hbm.at[token_rows(which)], x_ref.at[token_rows(which)])
+        load(("bu", n), bu_hbm.at[token_rows(which)], bu_ref.at[token_rows(which)])
+    load("qu", qu_hbm, qu_ref)
+    load("ku", ku_hbm, ku_ref)
+    load("h", h_hbm, h_ref)
+    if early < rows_in:
+        rest = pl.ds(early, rows_in - early)
+        load("mq2", mq_hbm.at[rest], mq_ref.at[rest])
+    for name, source, target in (
+        ("qf", qf_hbm, qf_ref), ("qs", qs_hbm, qs_ref), ("kf", kf_hbm, kf_ref), ("ks", ks_hbm, ks_ref),
+        ("qb", qb_hbm, qb_ref), ("kb", kb_hbm, kb_ref), ("mk", mk_hbm, mk_ref),
+        ("bf", bf_hbm, bf_ref), ("bs", bs_hbm, bs_ref), ("mb", mb_hbm, mb_ref),
+    ):
+        load(name, source, target)
+
+    greet(nf, nt, row, col, True)
+    sender = Sender(send_sem, recv_sem)
+    pair = {"fs": row, "tp": height * 2 + (1 - core)}
+    side, front, names = square(row, col)
+
+    def above(o):
+        return {"fs": row, "tp": lax.rem(height + o, nz) * 2 + core}
+
+    def beside(o):
+        return {"fs": lax.rem(row + o, nf), "tp": col}
+
+    parts = (first, second)
+    sent = []
+    for turn in range(2):
+        if turn == 0:
+            for n in range(2):
+                loads[f"mq{n}"].wait()
+                enc[parts[n], :] = coded(mq_ref[parts[n], :] * MASTER_GAIN, MASTER_POWER)
+        for n in range(2):
+            rows = parts[turn ^ n]
+            sent.append(sender.start(enc.at[rows], far.at[row, rows], names[n]))
+
+    for n in range(3):
+        loads["own", n].wait()
+        turned[n * rank : (n + 1) * rank, :] = own_ref[n].T
+
+    def project(n, which):
+        loads["x", n].wait()
+        loads["bu", n].wait()
+        over = (((1,), (1,)), ((), ()))
+        a = lax.dot_general(turned[: 2 * rank, :], x_ref[token_rows(which), :], over, preferred_element_type=jnp.float32)
+        b = lax.dot_general(turned[2 * rank :, :], bu_ref[token_rows(which), :], over, preferred_element_type=jnp.float32)
+        return a, b
+
+    a, b = project(0, 1 - core)
+    part[: 2 * rank, :] = a
+    part[2 * rank :, :] = b
+    swap = sender.start(part, from_pair, pair)
+    a, b = project(1, core)
+    swap.wait_recv()
+    for n in range(nz):
+        span = slice(n * piece, (n + 1) * piece)
+        halves[n, : 2 * rank, :] = a[:, span] + from_pair[: 2 * rank, span]
+        halves[n, 2 * rank :, :] = b[:, span] + from_pair[2 * rank :, span]
+
+    def put(target, n, values):
+        for k in range(3):
+            codes, scale = pack_columns(values[k * rank : (k + 1) * rank])
+            target[n, k * rank : (k + 1) * rank, :] = codes
+            target[n, 3 * rank + 16 * k : 3 * rank + 16 * (k + 1), :] = scale
+
+    def take(source, n, k):
+        return unpack_columns(
+            source[n, k * rank : (k + 1) * rank, :],
+            source[n, 3 * rank + 16 * k : 3 * rank + 16 * (k + 1), :],
+        )
+
+    copies = []
+    for o in range(1, nz):
+        to = lax.rem(height + o, nz)
+        put(sent_z, to, halves[to])
+        copies.append(sender.start(sent_z.at[to], arrived.at[o - 1], above(o)))
+    for copy in copies:
+        copy.wait_recv()
+    for k in range(3):
+        span = slice(k * rank, (k + 1) * rank)
+        total = halves[height, span, :]
+        for o in range(nz - 1):
+            total = total + take(arrived, o, k)
+        codes, scale = pack_columns(total)
+        whole[height, span, :] = codes
+        whole[height, 3 * rank + 16 * k : 3 * rank + 16 * (k + 1), :] = scale
+    copies = [sender.start(whole.at[height], whole.at[height], above(o)) for o in range(1, nz)]
+    across = [sender.start(whole.at[height], other.at[height], pair)]
+
+    passed = []
+    for n, source in ((0, side), (1, front)):
+        sent[n].wait_recv()
+        held = far.at[source, parts[n]]
+        passed.append(sender.start(held, held, names[1 - n]))
+
+    bbt_ref[...] = turned[2 * rank :, :]
+    for o, copy in enumerate(copies, 1):
+        copy.wait_recv()
+        source = lax.rem(height + nz - o, nz)
+        across.append(sender.start(whole.at[source], other.at[source], pair))
+
+    def low_parts(held, which):
+        for n in range(nz):
+            for k in range(3):
+                high, low = split_two(take(held, n, k))
+                split_ref[k, :rank, n * piece : (n + 1) * piece] = high
+                split_ref[k, rank:, n * piece : (n + 1) * piece] = low
+        lows = []
+        for k, ref in enumerate((qu_ref, ku_ref, h_ref)):
+            both = jnp.dot(split_ref[k], ref[token_rows(which), :], preferred_element_type=jnp.float32)
+            lows.append(both[:rank] + both[rank:])
+        return lows
+
+    for name in ("qu", "ku", "h"):
+        loads[name].wait()
+    one = low_parts(whole, core)
+    for copy in across:
+        copy.wait_recv()
+    two = low_parts(other, 1 - core)
+    thin, wide = rank // nf, features // nf
+    query_part, key_part, branch_part = [a + b for a, b in zip(one, two)]
+    part_qk[:, :, :query_cols] = query_part.reshape(nf, thin, query_cols)
+    part_qk[:, :, query_cols:] = key_part.reshape(nf, thin, key_cols)
+    for n in range(nf):
+        part_b[n] = branch_part[:, n * wide : (n + 1) * wide]
+
+    copies = []
+    for o in range(1, nf):
+        to = lax.rem(row + o, nf)
+        copies.append(sender.start(part_qk.at[to], got_qk.at[o - 1], beside(o)))
+        copies.append(sender.start(part_b.at[to], got_b.at[o - 1], beside(o)))
+    for copy in copies:
+        copy.wait_recv()
+    sum_qk, sum_b = part_qk[row], part_b[row]
+    for o in range(nf - 1):
+        sum_qk = sum_qk + got_qk[o]
+        sum_b = sum_b + got_b[o]
+    squares = jnp.sum(sum_qk * sum_qk) + jnp.sum(sum_b * sum_b)
+    sums_f[row] = jnp.full((8, 128), squares, jnp.float32)
+    copies_s = [sender.start(sums_f.at[row], sums_f.at[row], beside(o)) for o in range(1, nf)]
+    all_qk[row] = sum_qk
+    copies_qk = [sender.start(all_qk.at[row], all_qk.at[row], beside(o)) for o in range(1, nf)]
+    sum_b = sum_b.T
+    codes, scale = pack_columns(sum_b)
+    own_b[:wide, :] = codes
+    own_b[wide:, :] = scale
+
+    spread = sender.reserve(nz - 1)
+    to_owner = sender.reserve(1)
+    owner = {"fs": height, "tp": col}
+
+    def to_block(source, target):
+        return pltpu.make_async_remote_copy(
+            src_ref=source, dst_ref=target, send_sem=send_sem.at[to_owner], recv_sem=b_recv.at[row],
+            device_id=owner, device_id_type=pl.DeviceIdType.MESH,
+        )
+
+    @pl.when(row != height)
+    def _():
+        to_block(own_b, blocks_b.at[row]).start()
+
+    for copy in copies_s:
+        copy.wait_recv()
+    sums_t[col] = jnp.sum(sums_f[...], axis=0)
+    copies_s = [
+        sender.start(sums_t.at[col], sums_t.at[col], {"fs": row, "tp": lax.rem(col + o, nt)})
+        for o in range(1, nt)
+    ]
+
+    def spread_copy(o):
+        return pltpu.make_async_remote_copy(
+            src_ref=blocks_b, dst_ref=blocks_b, send_sem=send_sem.at[spread + o - 1], recv_sem=b_recv.at[nf],
+            device_id=above(o), device_id_type=pl.DeviceIdType.MESH,
+        )
+
+    @pl.when(row == height)
+    def _():
+        blocks_b[row] = own_b[...]
+        for o in range(1, nf):
+            source = lax.rem(row + o, nf)
+            pltpu.make_async_remote_copy(
+                src_ref=own_b, dst_ref=blocks_b.at[source], send_sem=send_sem.at[to_owner],
+                recv_sem=b_recv.at[source], device_id=owner, device_id_type=pl.DeviceIdType.MESH,
+            ).wait_recv()
+        for o in range(1, nz):
+            spread_copy(o).start()
+
+    for copy in copies_qk:
+        copy.wait_recv()
+    for name in ("qf", "qs", "kf", "ks", "qb", "kb", "mk") + (("mq2",) if early < rows_in else ()):
+        loads[name].wait()
+    for copy in copies_s:
+        copy.wait_recv()
+    total = jnp.sum(sums_t[...], axis=0)[0:1, 0:1]
+    entries = rank * nt * (2 * query_cols + key_cols)
+    clip = 1.0 / jnp.maximum(1.0, jnp.sqrt(total / float(entries)) / CLIP_RMS)
+
+    lows = all_qk[...].reshape(rank, query_cols + key_cols)
+    qf_out[...], qs_out[...], q_dir = moments(qf_ref[...], qs_ref[...], lows[:, :query_cols], clip)
+    kf_out[...], ks_out[...], k_dir = moments(kf_ref[...], ks_ref[...], lows[:, query_cols:], clip)
+    q_terms, k_terms = split_two(q_dir), split_two(k_dir)
+    late = []
+
+    def send_block(out, base, count):
+        part_rows = count // 2
+        for h in range(2):
+            target = pl.ds(base + h * part_rows, part_rows)
+            for n in ((0, 1), (1, 0))[h]:
+                held = out.at[row, target]
+                late.append((n, h, out, target, sender.start(held, held, names[n])))
+
+    def basis_rows(ref, source, base, count):
+        return ref[pl.ds(pl.multiple_of(source * rows_in + base, 16), count), :]
+
+    def own_update(step_ref, new_ref, out, master, basis, terms, base, count):
+        rows = slice(base, base + count)
+        step = exact_dot(basis_rows(basis, row, base, count), terms)
+        step_ref[rows, :] = step
+        updated = master[rows, :] - LEARN * step
+        new_ref[rows, :] = updated
+        out[row, rows, :] = updated.astype(out.dtype)
+
+    if early < rows_in:
+        own_update(q_step, q_new, q_out, mq_ref, qb_ref, q_terms, early, rows_in - early)
+        send_block(q_out, early, rows_in - early)
+    own_update(k_step, k_new, k_out, mk_ref, kb_ref, k_terms, 0, rows_in)
+    send_block(k_out, 0, rows_in)
+
+    @pl.when(row != height)
+    def _():
+        spread_copy(1).wait_recv()
+
+    swap_b = sender.start(blocks_b, pair_b, pair)
+    for name in ("bf", "bs", "mb"):
+        loads[name].wait()
+    swap_b.wait_recv()
+
+    def branch_low(held):
+        return [unpack_columns(held[n, :wide, :], held[n, wide:, :]) for n in range(nf)]
+
+    mine, theirs = branch_low(blocks_b), branch_low(pair_b)
+    for place in range(2):
+        here = core == place
+        for n in range(nf):
+            low = jnp.where(here, mine[n], theirs[n])
+            rows = slice(place * features + n * wide, place * features + (n + 1) * wide)
+            bf_out[rows, :], bs_out[rows, :], b_dir = moments(bf_ref[rows, :], bs_ref[rows, :], low, clip)
+            step = sum(
+                jnp.dot(term, bbt_ref[...], preferred_element_type=jnp.float32)
+                for term in split_two(b_dir)
+            )
+            b_step[rows, :] = step
+            updated = mb_ref[rows, :] - LEARN * step
+            b_new[rows, :] = updated
+            b_out[row, rows, :] = updated.astype(b_out.dtype)
+    send_block(b_out, 0, rows_in)
+
+    own_update(q_step, q_new, q_out, mq_ref, qb_ref, q_terms, 0, early)
+    for copy in sent[2:] + passed:
+        copy.wait_recv()
+    for o in range(1, nf):
+        source = lax.rem(row + o, nf)
+        step = exact_dot(basis_rows(qb_ref, source, 0, early), q_terms)
+        master = decoded(far[source], MASTER_POWER) * (1.0 / MASTER_GAIN)
+        q_out[source, :early, :] = (master - LEARN * step).astype(q_out.dtype)
+
+    last = []
+    for n, h, out, target, copy in late:
+        copy.wait_recv()
+        if n == h:
+            held = out.at[(side, front)[n], target]
+            last.append(sender.start(held, held, names[1 - n]))
+    for copy in last:
+        copy.wait_recv()
+    sender.drain()
+
+    @pl.when(row != height)
+    def _():
+        to_block(own_b, blocks_b.at[row]).wait_send()
+
+    @pl.when(row == height)
+    def _():
+        for o in range(1, nz):
+            spread_copy(o).wait_send()
+
+
+def fused(nf, nt, early, *args):
+    x, qu, ku, h, bu, mq, mk, mb, qb, kb, bb, qf, qs, kf, ks, bf, bs = args
+    tokens, features = x.shape
+    rank = qb.shape[1]
+    half, nz = tokens // 2, nt // 2
+    piece, thin, wide = half // nz, rank // nf, features // nf
+    cols = qu.shape[1] + ku.shape[1]
+    coded_rows = 3 * rank + 48
+    count = 80
+    f32, b16 = jnp.float32, jnp.bfloat16
+    vmem = pltpu.VMEM
+    outs = [vmem(m.shape, f32) for m in (mq, mk, mb)] * 2
+    outs += [vmem((nf, *m.shape), b16) for m in (mq, mk, mb)]
+    outs += [vmem(m.shape, f32) for m in (qf, qs, kf, ks, bf, bs)]
+    held = (x, qu, ku, h, bu, mq, mk, mb, qb, kb, qf, qs, kf, ks, bf, bs)
+    results = pl.pallas_call(
+        functools.partial(fused_kernel, nf, nt, early),
+        out_shape=tuple(outs),
+        in_specs=[pl.BlockSpec(memory_space=pl.ANY)] * len(args),
+        out_specs=(pl.BlockSpec(memory_space=pltpu.VMEM),) * len(outs),
+        scratch_shapes=[
+            *[vmem(a.shape, a.dtype) for a in held],
+            vmem((3, features, rank), b16),
+            vmem((3 * rank, features), b16),
+            vmem((rank, features), b16),
+            vmem((3 * rank, half), f32),
+            vmem((3 * rank, half), f32),
+            vmem((nz, 3 * rank, piece), f32),
+            vmem((nz, coded_rows, piece), b16),
+            vmem((nz - 1, coded_rows, piece), b16),
+            vmem((nz, coded_rows, piece), b16),
+            vmem((nz, coded_rows, piece), b16),
+            vmem((3, 2 * rank, half), b16),
+            vmem((nf, thin, cols), f32),
+            vmem((nf, rank, wide), f32),
+            vmem((nf - 1, thin, cols), f32),
+            vmem((nf - 1, rank, wide), f32),
+            vmem((nf, thin, cols), f32),
+            vmem((wide + 16, rank), b16),
+            vmem((nf, wide + 16, rank), b16),
+            vmem((nf, wide + 16, rank), b16),
+            vmem((nf, 8, 128), f32),
+            vmem((nt, 8, 128), f32),
+            vmem((early, mq.shape[1]), b16),
+            vmem((nf, early, mq.shape[1]), b16),
+            pltpu.SemaphoreType.DMA((count,)),
+            pltpu.SemaphoreType.DMA((count,)),
+            pltpu.SemaphoreType.DMA((32,)),
+            pltpu.SemaphoreType.DMA((nf + 1,)),
+        ],
+        compiler_params=pltpu.CompilerParams(
+            collective_id=0, has_side_effects=True, vmem_limit_bytes=VMEM_LIMIT
+        ),
+    )(*args)
+    results = list(results)
+    results[6:9] = [r.reshape(-1, r.shape[-1]) for r in results[6:9]]
+    return tuple(results)
+
+
 def per_device(
     normed_inputs,
     query_upstream,
@@ -431,6 +876,15 @@
     key_local = key_upstream.shape[1]
     rows_in = query_master.shape[0]
     rank = query_basis.shape[1]
+    even = n_cols == 2 * n_rows and features * 2 == rows_in and key_local % 128 == 0
+    if n_rows == 4 and even and features % 512 == 0 and normed_inputs.shape[0] % 1024 == 0:
+        return fused(
+            n_rows, n_cols, rows_in // 64 * EARLY_OF_64, normed_inputs, query_upstream, key_upstream,
+            head_outputs, branch_upstream, query_master, key_master, branch_master,
+            query_basis, key_basis, branch_basis, query_first, query_second,
+            key_first, key_second, branch_first, branch_second,
+        )
+
     def own_block(basis):
         return lax.dynamic_slice_in_dim(basis, col_index * features, features, 0)
 

time: 164 us -> 120 us (0.73); the launches traced: 161 us -> 120 us
  Pallas kernels: 135 us -> 103 us
  matrix products: 8.42 us -> 0 us
  other arithmetic: 4.05 us -> 0 us
  local copies, waits for them, and re-layouts: 12.3 us -> 16.1 us
    pallas_call x2 -> x1, Pallas kernels: 135 us -> 103 us  [fused(): pl.pallas_call(functools.partial(fused_kernel, nf, nt, early), out_shape=...]
    dot_general x3 -> x0, matrix products: 8.42 us -> none  [the longest x1 3.17 us: per_device(): branch_step = jnp.dot(b_dir, own_branch.T, precision=exact)]
    unnamed x37 -> x15, local copies, waits for them, and re-layouts: 7.71 us -> 16.1 us
    dynamic_slice x2 -> x0, local copies, waits for them, and re-layouts: 3.26 us -> none  [own_block(): return lax.dynamic_slice_in_dim(basis, col_index * features, features, 0)]
    div x1 -> x0, other arithmetic: 1.95 us -> none  [moments(): first_new / (jnp.sqrt(second_new) + ADAM_EPS)]
where the time goes in v1:
time: 120 us
  Pallas kernels  103 us (86%)
  local copies, waits for them, and re-layouts  16.1 us (13%)
    pallas_call x1, Pallas kernels, fused(): pl.pallas_call(functools.partial(fused_kernel, nf, nt, early), out_shape=...  103 us
    unnamed x15, local copies, waits for them, and re-layouts  16.1 us

profile of v1, /device:TPU:27, one launch (start us, length us, event | category | flops | bytes accessed | tf_op | source)
XLA Modules:
  0.0 120.1 jit_solution(2716952848068061806)
XLA Ops:
  0.7 103.3 %shard_map.280 = (f32[1024,512]{1,0:T(8,128)S(1)}, f32[1024,128]{1,0:T(8,128)S(1)}, f32[1024,512]{1,0:T(8,128)S(1)}, f32[1024,512]{1,0:T(8,128)S(1)}, f32[1024,1...) custom-call(bf16[1024,512]{1,0:T(8,128)(2,1)} %x_hbm.1, ...), custom_call_target="tpu_custom_call" | custom-call | tf_op jit(solution)/shard_map/pallas_call | solution.py:806
  104.0 1.3 %copy.47 = f32[1024,512]{1,0:T(8,128)} copy(f32[1024,512]{1,0:T(8,128)S(1)} %get-tuple-element.45) | data formatting | bytes 4194304
  105.3 0.6 copy.58
  105.9 0.6 copy.59
  106.6 0.7 copy.56
  107.3 0.7 copy.57
  108.0 0.8 copy.48
  108.8 0.8 copy.51
  109.5 0.8 copy.60
  110.3 0.8 copy.61
  111.1 1.0 copy.54
  112.1 1.3 %copy.49 = f32[1024,512]{1,0:T(8,128)} copy(f32[1024,512]{1,0:T(8,128)S(1)} %get-tuple-element.47) | data formatting | bytes 4194304
  113.4 1.3 %copy.50 = f32[1024,512]{1,0:T(8,128)} copy(f32[1024,512]{1,0:T(8,128)S(1)} %get-tuple-element.48) | data formatting | bytes 4194304
  114.7 1.3 %copy.52 = f32[1024,512]{1,0:T(8,128)} copy(f32[1024,512]{1,0:T(8,128)S(1)} %get-tuple-element.50) | data formatting | bytes 4194304
  116.1 2.0 %copy.53 = bf16[4096,512]{1,0:T(8,128)(2,1)} copy(bf16[4096,512]{1,0:T(8,128)(2,1)S(1)} %bitcast.4) | data formatting | bytes 8388608
  118.1 2.0 %copy.55 = bf16[4096,512]{1,0:T(8,128)(2,1)} copy(bf16[4096,512]{1,0:T(8,128)(2,1)S(1)} %bitcast.3) | data formatting | bytes 8388608

commit v2 on v1

--- a/solution.py
+++ b/solution.py
@@ -406,7 +406,8 @@
     return [out.reshape(-1, out.shape[-1]) for out in outs]
 
 
-EARLY_OF_64 = 56
+EARLY_OF_64 = 64
+PASSED_OF_16 = (8, 12)
 VMEM_LIMIT = 40 * 2**20
 MASTER_MOST = 0.09375
 MASTER_POWER = 14
@@ -438,19 +439,31 @@
     return jnp.where(codes < 0, -root, root)
 
 
-def column_scale(values):
-    most = jnp.max(jnp.abs(values), axis=0, keepdims=True)
-    return jnp.maximum(most, 1e-30).astype(jnp.bfloat16)
+def pack(values, axis):
+    most = jnp.max(jnp.abs(values), axis=axis, keepdims=True)
+    scale = jnp.maximum(most, 1e-30).astype(jnp.bfloat16).astype(jnp.float32)
+    return coded(values * (SUM_GAIN / scale), SUM_POWER), scale
+
+
+def unpack(codes, scale):
+    return decoded(codes, SUM_POWER) * (scale.astype(jnp.float32) * (1.0 / SUM_GAIN))
 
 
 def pack_columns(values):
-    scale = column_scale(values)
-    codes = coded(values * (SUM_GAIN / scale.astype(jnp.float32)), SUM_POWER)
-    return codes, jnp.broadcast_to(scale, (16, values.shape[1]))
+    codes, scale = pack(values, 0)
+    return codes, jnp.broadcast_to(scale, (16, values.shape[1])).astype(jnp.bfloat16)
 
 
 def unpack_columns(codes, scale):
-    return decoded(codes, SUM_POWER) * (scale[0:1].astype(jnp.float32) * (1.0 / SUM_GAIN))
+    return unpack(codes, scale[0:1])
+
+
+def stacked(scales, width):
+    place = lax.broadcasted_iota(jnp.int32, (16, width), 0)
+    rows = jnp.broadcast_to(scales[-1], (16, width))
+    for n, scale in enumerate(scales[:-1]):
+        rows = jnp.where(place == n, scale, rows)
+    return rows.astype(jnp.bfloat16)
 
 
 def split_two(values):
@@ -471,7 +484,7 @@
     x_ref, qu_ref, ku_ref, h_ref, bu_ref, mq_ref, mk_ref, mb_ref, qb_ref, kb_ref,
     qf_ref, qs_ref, kf_ref, ks_ref, bf_ref, bs_ref, own_ref, turned, bbt_ref,
     part, from_pair, halves, sent_z, arrived, whole, other, split_ref,
-    part_qk, part_b, got_qk, got_b, all_qk, own_b, blocks_b, pair_b, sums_f, sums_t,
+    part_qk, part_b, sent_qk, sent_b, got_qk, got_b, all_qk, own_b, blocks_b, pair_b, sums_f, sums_t,
     enc, far,
     send_sem, recv_sem, load_sem, b_recv,
 ):
@@ -490,6 +503,14 @@
         copy = pltpu.make_async_copy(source, target, load_sem.at[len(loads)])
         copy.start()
         loads[name] = copy
+
+    needed = set()
+
+    def need(*keys):
+        for key in keys:
+            if key not in needed:
+                needed.add(key)
+                loads[key].wait()
 
     def token_rows(which):
         return pl.ds(pl.multiple_of(which * half, half), half)
@@ -532,19 +553,18 @@
     for turn in range(2):
         if turn == 0:
             for n in range(2):
-                loads[f"mq{n}"].wait()
+                need(f"mq{n}")
                 enc[parts[n], :] = coded(mq_ref[parts[n], :] * MASTER_GAIN, MASTER_POWER)
         for n in range(2):
             rows = parts[turn ^ n]
             sent.append(sender.start(enc.at[rows], far.at[row, rows], names[n]))
 
     for n in range(3):
-        loads["own", n].wait()
+        need(("own", n))
         turned[n * rank : (n + 1) * rank, :] = own_ref[n].T
 
     def project(n, which):
-        loads["x", n].wait()
-        loads["bu", n].wait()
+        need(("x", n), ("bu", n))
         over = (((1,), (1,)), ((), ()))
         a = lax.dot_general(turned[: 2 * rank, :], x_ref[token_rows(which), :], over, preferred_element_type=jnp.float32)
         b = lax.dot_general(turned[2 * rank :, :], bu_ref[token_rows(which), :], over, preferred_element_type=jnp.float32)
@@ -562,40 +582,46 @@
         halves[n, 2 * rank :, :] = b[:, span] + from_pair[2 * rank :, span]
 
     def put(target, n, values):
+        scales = []
         for k in range(3):
-            codes, scale = pack_columns(values[k * rank : (k + 1) * rank])
+            codes, scale = pack(values[k], 0)
             target[n, k * rank : (k + 1) * rank, :] = codes
-            target[n, 3 * rank + 16 * k : 3 * rank + 16 * (k + 1), :] = scale
+            scales.append(scale)
+        target[n, 3 * rank :, :] = stacked(scales, piece)
 
     def take(source, n, k):
-        return unpack_columns(
-            source[n, k * rank : (k + 1) * rank, :],
-            source[n, 3 * rank + 16 * k : 3 * rank + 16 * (k + 1), :],
-        )
+        scale = source[n, 3 * rank :, :].astype(jnp.float32)[k : k + 1]
+        return unpack(source[n, k * rank : (k + 1) * rank, :], scale)
+
+    def thirds(values):
+        return [values[k * rank : (k + 1) * rank] for k in range(3)]
 
     copies = []
     for o in range(1, nz):
         to = lax.rem(height + o, nz)
-        put(sent_z, to, halves[to])
+        put(sent_z, to, thirds(halves[to]))
         copies.append(sender.start(sent_z.at[to], arrived.at[o - 1], above(o)))
     for copy in copies:
         copy.wait_recv()
+    totals = thirds(halves[height])
     for k in range(3):
-        span = slice(k * rank, (k + 1) * rank)
-        total = halves[height, span, :]
         for o in range(nz - 1):
-            total = total + take(arrived, o, k)
-        codes, scale = pack_columns(total)
-        whole[height, span, :] = codes
-        whole[height, 3 * rank + 16 * k : 3 * rank + 16 * (k + 1), :] = scale
+            totals[k] = totals[k] + take(arrived, o, k)
+    put(whole, height, totals)
     copies = [sender.start(whole.at[height], whole.at[height], above(o)) for o in range(1, nz)]
     across = [sender.start(whole.at[height], other.at[height], pair)]
 
     passed = []
-    for n, source in ((0, side), (1, front)):
+
+    def pass_on(begin, end):
+        unit = early // 32
+        for n, source in ((0, side), (1, front)):
+            held = far.at[source, pl.ds(n * (early // 2) + begin * unit, (end - begin) * unit)]
+            passed.append(sender.start(held, held, names[1 - n]))
+
+    for n in range(2):
         sent[n].wait_recv()
-        held = far.at[source, parts[n]]
-        passed.append(sender.start(held, held, names[1 - n]))
+    pass_on(0, PASSED_OF_16[0])
 
     bbt_ref[...] = turned[2 * rank :, :]
     for o, copy in enumerate(copies, 1):
@@ -615,34 +641,54 @@
             lows.append(both[:rank] + both[rank:])
         return lows
 
-    for name in ("qu", "ku", "h"):
-        loads[name].wait()
+    need("qu", "ku", "h")
     one = low_parts(whole, core)
     for copy in across:
         copy.wait_recv()
     two = low_parts(other, 1 - core)
     thin, wide = rank // nf, features // nf
     query_part, key_part, branch_part = [a + b for a, b in zip(one, two)]
+    cols = query_cols + key_cols
+
+    def put_qk(query, key):
+        query_codes, query_scale = pack(query, 1)
+        key_codes, key_scale = pack(key, 1)
+        place = lax.broadcasted_iota(jnp.int32, (query.shape[0], 128), 1)
+        scale = jnp.where(place < 64, query_scale, key_scale).astype(jnp.bfloat16)
+        return ((slice(0, query_cols), query_codes), (slice(query_cols, cols), key_codes), (slice(cols, cols + 128), scale))
+
+    def take_qk(held):
+        scale = held[:, cols:].astype(jnp.float32)
+        return unpack(held[:, :query_cols], scale[:, 0:1]), unpack(held[:, query_cols:cols], scale[:, 64:65])
+
+    for span, values in put_qk(query_part, key_part):
+        sent_qk[:, :, span] = values.reshape(nf, thin, values.shape[1])
     part_qk[:, :, :query_cols] = query_part.reshape(nf, thin, query_cols)
     part_qk[:, :, query_cols:] = key_part.reshape(nf, thin, key_cols)
+    codes, scale = pack_columns(branch_part)
     for n in range(nf):
         part_b[n] = branch_part[:, n * wide : (n + 1) * wide]
+        sent_b[n, :rank, :] = codes[:, n * wide : (n + 1) * wide]
+        sent_b[n, rank:, :] = scale[:, n * wide : (n + 1) * wide]
 
     copies = []
     for o in range(1, nf):
         to = lax.rem(row + o, nf)
-        copies.append(sender.start(part_qk.at[to], got_qk.at[o - 1], beside(o)))
-        copies.append(sender.start(part_b.at[to], got_b.at[o - 1], beside(o)))
+        copies.append(sender.start(sent_qk.at[to], got_qk.at[o - 1], beside(o)))
+        copies.append(sender.start(sent_b.at[to], got_b.at[o - 1], beside(o)))
+    pass_on(*PASSED_OF_16)
     for copy in copies:
         copy.wait_recv()
-    sum_qk, sum_b = part_qk[row], part_b[row]
+    sum_q, sum_k, sum_b = part_qk[row, :, :query_cols], part_qk[row, :, query_cols:], part_b[row]
     for o in range(nf - 1):
-        sum_qk = sum_qk + got_qk[o]
-        sum_b = sum_b + got_b[o]
-    squares = jnp.sum(sum_qk * sum_qk) + jnp.sum(sum_b * sum_b)
+        got_query, got_key = take_qk(got_qk[o])
+        sum_q, sum_k = sum_q + got_query, sum_k + got_key
+        sum_b = sum_b + unpack_columns(got_b[o, :rank, :], got_b[o, rank:, :])
+    squares = jnp.sum(sum_q * sum_q) + jnp.sum(sum_k * sum_k) + jnp.sum(sum_b * sum_b)
     sums_f[row] = jnp.full((8, 128), squares, jnp.float32)
     copies_s = [sender.start(sums_f.at[row], sums_f.at[row], beside(o)) for o in range(1, nf)]
-    all_qk[row] = sum_qk
+    for span, values in put_qk(sum_q, sum_k):
+        all_qk[row, :, span] = values
     copies_qk = [sender.start(all_qk.at[row], all_qk.at[row], beside(o)) for o in range(1, nf)]
     sum_b = sum_b.T
     codes, scale = pack_columns(sum_b)
@@ -663,6 +709,7 @@
     def _():
         to_block(own_b, blocks_b.at[row]).start()
 
+    pass_on(PASSED_OF_16[1], 16)
     for copy in copies_s:
         copy.wait_recv()
     sums_t[col] = jnp.sum(sums_f[...], axis=0)
@@ -691,17 +738,18 @@
 
     for copy in copies_qk:
         copy.wait_recv()
-    for name in ("qf", "qs", "kf", "ks", "qb", "kb", "mk") + (("mq2",) if early < rows_in else ()):
-        loads[name].wait()
+    need("qf", "qs", "kf", "ks", "qb", "kb", "mk")
+    if early < rows_in:
+        need("mq2")
     for copy in copies_s:
         copy.wait_recv()
     total = jnp.sum(sums_t[...], axis=0)[0:1, 0:1]
     entries = rank * nt * (2 * query_cols + key_cols)
     clip = 1.0 / jnp.maximum(1.0, jnp.sqrt(total / float(entries)) / CLIP_RMS)
 
-    lows = all_qk[...].reshape(rank, query_cols + key_cols)
-    qf_out[...], qs_out[...], q_dir = moments(qf_ref[...], qs_ref[...], lows[:, :query_cols], clip)
-    kf_out[...], ks_out[...], k_dir = moments(kf_ref[...], ks_ref[...], lows[:, query_cols:], clip)
+    query_low, key_low = take_qk(all_qk[...].reshape(rank, cols + 128))
+    qf_out[...], qs_out[...], q_dir = moments(qf_ref[...], qs_ref[...], query_low, clip)
+    kf_out[...], ks_out[...], k_dir = moments(kf_ref[...], ks_ref[...], key_low, clip)
     q_terms, k_terms = split_two(q_dir), split_two(k_dir)
     late = []
 
@@ -735,8 +783,7 @@
         spread_copy(1).wait_recv()
 
     swap_b = sender.start(blocks_b, pair_b, pair)
-    for name in ("bf", "bs", "mb"):
-        loads[name].wait()
+    need("bf", "bs", "mb")
     swap_b.wait_recv()
 
     def branch_low(held):
@@ -788,6 +835,27 @@
             spread_copy(o).wait_send()
 
 
+def flush_kernel(*refs):
+    count = len(refs) // 2
+    copies = []
+    for n in range(count):
+        copies.append(pltpu.make_async_copy(refs[n], refs[count + n], refs[-1].at[n]))
+        copies[-1].start()
+    for copy in copies:
+        copy.wait()
+
+
+def flushed(results):
+    return pl.pallas_call(
+        flush_kernel,
+        out_shape=tuple(jax.ShapeDtypeStruct(r.shape, r.dtype) for r in results),
+        in_specs=[pl.BlockSpec(memory_space=pltpu.VMEM)] * len(results),
+        out_specs=(pl.BlockSpec(memory_space=pl.ANY),) * len(results),
+        scratch_shapes=[pltpu.SemaphoreType.DMA((len(results),))],
+        compiler_params=pltpu.CompilerParams(vmem_limit_bytes=2**20),
+    )(*results)
+
+
 def fused(nf, nt, early, *args):
     x, qu, ku, h, bu, mq, mk, mb, qb, kb, bb, qf, qs, kf, ks, bf, bs = args
     tokens, features = x.shape
@@ -795,7 +863,7 @@
     half, nz = tokens // 2, nt // 2
     piece, thin, wide = half // nz, rank // nf, features // nf
     cols = qu.shape[1] + ku.shape[1]
-    coded_rows = 3 * rank + 48
+    coded_rows = 3 * rank + 16
     count = 80
     f32, b16 = jnp.float32, jnp.bfloat16
     vmem = pltpu.VMEM
@@ -823,9 +891,11 @@
             vmem((3, 2 * rank, half), b16),
             vmem((nf, thin, cols), f32),
             vmem((nf, rank, wide), f32),
-            vmem((nf - 1, thin, cols), f32),
-            vmem((nf - 1, rank, wide), f32),
-            vmem((nf, thin, cols), f32),
+            vmem((nf, thin, cols + 128), b16),
+            vmem((nf, rank + 16, wide), b16),
+            vmem((nf - 1, thin, cols + 128), b16),
+            vmem((nf - 1, rank + 16, wide), b16),
+            vmem((nf, thin, cols + 128), b16),
             vmem((wide + 16, rank), b16),
             vmem((nf, wide + 16, rank), b16),
             vmem((nf, wide + 16, rank), b16),
@@ -842,7 +912,7 @@
             collective_id=0, has_side_effects=True, vmem_limit_bytes=VMEM_LIMIT
         ),
     )(*args)
-    results = list(results)
+    results = list(flushed(results))
     results[6:9] = [r.reshape(-1, r.shape[-1]) for r in results[6:9]]
     return tuple(results)
 

time: 120 us -> 105 us (0.88)
  local copies, waits for them, and re-layouts: 16.1 us -> 0 us
    unnamed x15 -> x0, local copies, waits for them, and re-layouts: 16.1 us -> none
    pallas_call x0 -> x1, Pallas kernels: none -> 7.11 us  [flushed(): pl.pallas_call(flush_kernel, out_shape=tuple((jax.ShapeDtypeStruct(r.shap...]
    pallas_call x1, Pallas kernels: 103 us -> 96.8 us  [fused(): pl.pallas_call(functools.partial(fused_kernel, nf, nt, early), out_shape=...]
where the time goes in v2:
time: 105 us
  Pallas kernels  104 us (99%)
    pallas_call x1, Pallas kernels, fused(): pl.pallas_call(functools.partial(fused_kernel, nf, nt, early), out_shape=...  96.8 us
    pallas_call x1, Pallas kernels, flushed(): pl.pallas_call(flush_kernel, out_shape=tuple((jax.ShapeDtypeStruct(r.shap...  7.11 us

profile of v2, /device:TPU:27, one launch (start us, length us, event | category | flops | bytes accessed | tf_op | source)
XLA Modules:
  0.0 104.5 jit_solution(2386005383568023213)
XLA Ops:
  0.7 96.8 %shard_map.280 = (f32[1024,512]{1,0:T(8,128)S(1)}, f32[1024,128]{1,0:T(8,128)S(1)}, f32[1024,512]{1,0:T(8,128)S(1)}, f32[1024,512]{1,0:T(8,128)S(1)}, f32[1024,1...) custom-call(bf16[1024,512]{1,0:T(8,128)(2,1)} %x_hbm.1, ...), custom_call_target="tpu_custom_call" | custom-call | tf_op jit(solution)/shard_map/pallas_call | solution.py:874
  97.4 7.1 %shard_map.281 = (f32[1024,512]{1,0:T(8,128)}, f32[1024,128]{1,0:T(8,128)}, f32[1024,512]{1,0:T(8,128)}, f32[1024,512]{1,0:T(8,128)}, f32[1024,128]{1,0:T(8,128)...) custom-call(f32[1024,512]{1,0:T(8,128)S(1)} %get-tuple-element.45.re, ...), custom_call_target="tpu_custom_call" | custom-call | tf_op jit(solution)/shard_map/pallas_call | solution.py:849

commit v3 on v2

--- a/solution.py
+++ b/solution.py
@@ -407,7 +407,9 @@
 
 
 EARLY_OF_64 = 64
-PASSED_OF_16 = (8, 12)
+PASSED_OF_16 = (9, 11)
+K_EARLY_OF_16 = 16
+KEY_LATER = False
 VMEM_LIMIT = 40 * 2**20
 MASTER_MOST = 0.09375
 MASTER_POWER = 14
@@ -485,7 +487,7 @@
     qf_ref, qs_ref, kf_ref, ks_ref, bf_ref, bs_ref, own_ref, turned, bbt_ref,
     part, from_pair, halves, sent_z, arrived, whole, other, split_ref,
     part_qk, part_b, sent_qk, sent_b, got_qk, got_b, all_qk, own_b, blocks_b, pair_b, sums_f, sums_t,
-    enc, far,
+    enc, far, enc_k, far_k,
     send_sem, recv_sem, load_sem, b_recv,
 ):
     row, col = lax.axis_index("fs"), lax.axis_index("tp")
@@ -498,6 +500,11 @@
     query_cols, key_cols = qu_ref.shape[1], ku_ref.shape[1]
     rows_in = mq_ref.shape[0]
     loads = {}
+    barrier = pltpu.get_barrier_semaphore()
+    peers = [{"fs": lax.rem(row + o, nf), "tp": col} for o in range(1, nf)]
+    peers += [{"fs": row, "tp": lax.rem(col + o, nt)} for o in range(1, nt)]
+    for peer in peers:
+        pl.semaphore_signal(barrier, inc=1, device_id=peer, device_id_type=pl.DeviceIdType.MESH)
 
     def load(name, source, target):
         copy = pltpu.make_async_copy(source, target, load_sem.at[len(loads)])
@@ -515,6 +522,7 @@
     def token_rows(which):
         return pl.ds(pl.multiple_of(which * half, half), half)
 
+    k_early = enc_k.shape[0]
     first, second = pl.ds(0, early // 2), pl.ds(early // 2, early // 2)
     load("mq0", mq_hbm.at[first], mq_ref.at[first])
     load("mq1", mq_hbm.at[second], mq_ref.at[second])
@@ -537,7 +545,6 @@
     ):
         load(name, source, target)
 
-    greet(nf, nt, row, col, True)
     sender = Sender(send_sem, recv_sem)
     pair = {"fs": row, "tp": height * 2 + (1 - core)}
     side, front, names = square(row, col)
@@ -549,16 +556,9 @@
         return {"fs": lax.rem(row + o, nf), "tp": col}
 
     parts = (first, second)
-    sent = []
-    for turn in range(2):
-        if turn == 0:
-            for n in range(2):
-                need(f"mq{n}")
-                enc[parts[n], :] = coded(mq_ref[parts[n], :] * MASTER_GAIN, MASTER_POWER)
-        for n in range(2):
-            rows = parts[turn ^ n]
-            sent.append(sender.start(enc.at[rows], far.at[row, rows], names[n]))
-
+    for n in range(2):
+        need(f"mq{n}")
+        enc[parts[n], :] = coded(mq_ref[parts[n], :] * MASTER_GAIN, MASTER_POWER)
     for n in range(3):
         need(("own", n))
         turned[n * rank : (n + 1) * rank, :] = own_ref[n].T
@@ -573,6 +573,12 @@
     a, b = project(0, 1 - core)
     part[: 2 * rank, :] = a
     part[2 * rank :, :] = b
+    pl.semaphore_wait(barrier, len(peers))
+    sent = []
+    for turn in range(2):
+        for n in range(2):
+            rows = parts[turn ^ n]
+            sent.append(sender.start(enc.at[rows], far.at[row, rows], names[n]))
     swap = sender.start(part, from_pair, pair)
     a, b = project(1, core)
     swap.wait_recv()
@@ -614,6 +620,8 @@
     passed = []
 
     def pass_on(begin, end):
+        if begin == end:
+            return
         unit = early // 32
         for n, source in ((0, side), (1, front)):
             held = far.at[source, pl.ds(n * (early // 2) + begin * unit, (end - begin) * unit)]
@@ -676,6 +684,26 @@
         to = lax.rem(row + o, nf)
         copies.append(sender.start(sent_qk.at[to], got_qk.at[o - 1], beside(o)))
         copies.append(sender.start(sent_b.at[to], got_b.at[o - 1], beside(o)))
+    need("mk")
+    enc_k[...] = coded(mk_ref[:k_early, :] * MASTER_GAIN, MASTER_POWER)
+    sent_k = []
+
+    def send_key():
+        for h in range(2):
+            rows = pl.ds(h * (k_early // 2), k_early // 2)
+            for n in ((0, 1), (1, 0))[h]:
+                copy = sender.start(enc_k.at[rows], far_k.at[row, rows], names[n])
+                sent_k.append((n, h, rows, copy))
+
+    def pass_key():
+        for n, h, rows, copy in sent_k:
+            copy.wait_recv()
+            if n == h:
+                held = far_k.at[(side, front)[n], rows]
+                passed.append(sender.start(held, held, names[1 - n]))
+
+    if not KEY_LATER:
+        send_key()
     pass_on(*PASSED_OF_16)
     for copy in copies:
         copy.wait_recv()
@@ -695,7 +723,7 @@
     own_b[:wide, :] = codes
     own_b[wide:, :] = scale
 
-    spread = sender.reserve(nz - 1)
+    spread = sender.reserve(nf * (nz - 1))
     to_owner = sender.reserve(1)
     owner = {"fs": height, "tp": col}
 
@@ -710,6 +738,10 @@
         to_block(own_b, blocks_b.at[row]).start()
 
     pass_on(PASSED_OF_16[1], 16)
+    if KEY_LATER:
+        send_key()
+    else:
+        pass_key()
     for copy in copies_s:
         copy.wait_recv()
     sums_t[col] = jnp.sum(sums_f[...], axis=0)
@@ -718,31 +750,35 @@
         for o in range(1, nt)
     ]
 
-    def spread_copy(o):
+    def spread_copy(turn, o):
+        held = blocks_b.at[lax.rem(row + turn, nf)]
         return pltpu.make_async_remote_copy(
-            src_ref=blocks_b, dst_ref=blocks_b, send_sem=send_sem.at[spread + o - 1], recv_sem=b_recv.at[nf],
-            device_id=above(o), device_id_type=pl.DeviceIdType.MESH,
+            src_ref=held, dst_ref=held, send_sem=send_sem.at[spread + turn * (nz - 1) + o - 1],
+            recv_sem=b_recv.at[nf + turn], device_id=above(o), device_id_type=pl.DeviceIdType.MESH,
         )
 
     @pl.when(row == height)
     def _():
         blocks_b[row] = own_b[...]
-        for o in range(1, nf):
-            source = lax.rem(row + o, nf)
-            pltpu.make_async_remote_copy(
-                src_ref=own_b, dst_ref=blocks_b.at[source], send_sem=send_sem.at[to_owner],
-                recv_sem=b_recv.at[source], device_id=owner, device_id_type=pl.DeviceIdType.MESH,
-            ).wait_recv()
-        for o in range(1, nz):
-            spread_copy(o).start()
+        for turn in range(nf):
+            source = lax.rem(row + turn, nf)
+            if turn:
+                pltpu.make_async_remote_copy(
+                    src_ref=own_b, dst_ref=blocks_b.at[source], send_sem=send_sem.at[to_owner],
+                    recv_sem=b_recv.at[source], device_id=owner, device_id_type=pl.DeviceIdType.MESH,
+                ).wait_recv()
+            for o in range(nz - 1, 0, -1):
+                spread_copy(turn, o).start()
 
     for copy in copies_qk:
         copy.wait_recv()
-    need("qf", "qs", "kf", "ks", "qb", "kb", "mk")
+    need("qf", "qs", "kf", "ks", "qb", "kb")
     if early < rows_in:
         need("mq2")
     for copy in copies_s:
         copy.wait_recv()
+    if KEY_LATER:
+        pass_key()
     total = jnp.sum(sums_t[...], axis=0)[0:1, 0:1]
     entries = rank * nt * (2 * query_cols + key_cols)
     clip = 1.0 / jnp.maximum(1.0, jnp.sqrt(total / float(entries)) / CLIP_RMS)
@@ -753,13 +789,16 @@
     q_terms, k_terms = split_two(q_dir), split_two(k_dir)
     late = []
 
-    def send_block(out, base, count):
+    def send_block(out, span, count):
         part_rows = count // 2
+
+        def target(source, h):
+            return out.at[source, pl.ds(pl.multiple_of(span(source) + h * part_rows, part_rows), part_rows)]
+
         for h in range(2):
-            target = pl.ds(base + h * part_rows, part_rows)
             for n in ((0, 1), (1, 0))[h]:
-                held = out.at[row, target]
-                late.append((n, h, out, target, sender.start(held, held, names[n])))
+                held = target(row, h)
+                late.append((n, h, target, sender.start(held, held, names[n])))
 
     def basis_rows(ref, source, base, count):
         return ref[pl.ds(pl.multiple_of(source * rows_in + base, 16), count), :]
@@ -774,52 +813,60 @@
 
     if early < rows_in:
         own_update(q_step, q_new, q_out, mq_ref, qb_ref, q_terms, early, rows_in - early)
-        send_block(q_out, early, rows_in - early)
-    own_update(k_step, k_new, k_out, mk_ref, kb_ref, k_terms, 0, rows_in)
-    send_block(k_out, 0, rows_in)
-
-    @pl.when(row != height)
-    def _():
-        spread_copy(1).wait_recv()
-
-    swap_b = sender.start(blocks_b, pair_b, pair)
+        send_block(q_out, lambda source: early, rows_in - early)
+    if k_early < rows_in:
+        own_update(k_step, k_new, k_out, mk_ref, kb_ref, k_terms, k_early, rows_in - k_early)
+        send_block(k_out, lambda source: k_early, rows_in - k_early)
     need("bf", "bs", "mb")
-    swap_b.wait_recv()
-
-    def branch_low(held):
-        return [unpack_columns(held[n, :wide, :], held[n, wide:, :]) for n in range(nf)]
-
-    mine, theirs = branch_low(blocks_b), branch_low(pair_b)
-    for place in range(2):
-        here = core == place
-        for n in range(nf):
-            low = jnp.where(here, mine[n], theirs[n])
-            rows = slice(place * features + n * wide, place * features + (n + 1) * wide)
-            bf_out[rows, :], bs_out[rows, :], b_dir = moments(bf_ref[rows, :], bs_ref[rows, :], low, clip)
-            step = sum(
-                jnp.dot(term, bbt_ref[...], preferred_element_type=jnp.float32)
-                for term in split_two(b_dir)
-            )
-            b_step[rows, :] = step
-            updated = mb_ref[rows, :] - LEARN * step
-            b_new[rows, :] = updated
-            b_out[row, rows, :] = updated.astype(b_out.dtype)
-    send_block(b_out, 0, rows_in)
-
+
+    def branch_rows(held, place, turn):
+        def span(source):
+            return place * features + lax.rem(source + turn, nf) * wide
+
+        source = lax.rem(row + turn, nf)
+        rows = pl.ds(pl.multiple_of(span(row), wide), wide)
+        low = unpack_columns(held[source, :wide, :], held[source, wide:, :])
+        bf_out[rows, :], bs_out[rows, :], b_dir = moments(bf_ref[rows, :], bs_ref[rows, :], low, clip)
+        step = sum(
+            jnp.dot(term, bbt_ref[...], preferred_element_type=jnp.float32)
+            for term in split_two(b_dir)
+        )
+        b_step[rows, :] = step
+        updated = mb_ref[rows, :] - LEARN * step
+        b_new[rows, :] = updated
+        b_out[row, rows, :] = updated.astype(b_out.dtype)
+        send_block(b_out, span, wide)
+
+    for turn in range(nf):
+        source = lax.rem(row + turn, nf)
+
+        @pl.when(row != height)
+        def _():
+            spread_copy(turn, 1).wait_recv()
+
+        swap_b = sender.start(blocks_b.at[source], pair_b.at[source], pair)
+        branch_rows(blocks_b, core, turn)
+        swap_b.wait_recv()
+        branch_rows(pair_b, 1 - core, turn)
+
+    own_update(k_step, k_new, k_out, mk_ref, kb_ref, k_terms, 0, k_early)
     own_update(q_step, q_new, q_out, mq_ref, qb_ref, q_terms, 0, early)
     for copy in sent[2:] + passed:
         copy.wait_recv()
     for o in range(1, nf):
         source = lax.rem(row + o, nf)
-        step = exact_dot(basis_rows(qb_ref, source, 0, early), q_terms)
-        master = decoded(far[source], MASTER_POWER) * (1.0 / MASTER_GAIN)
-        q_out[source, :early, :] = (master - LEARN * step).astype(q_out.dtype)
+        for held, count, basis, terms, out in (
+            (far_k, k_early, kb_ref, k_terms, k_out), (far, early, qb_ref, q_terms, q_out)
+        ):
+            step = exact_dot(basis_rows(basis, source, 0, count), terms)
+            master = decoded(held[source], MASTER_POWER) * (1.0 / MASTER_GAIN)
+            out[source, :count, :] = (master - LEARN * step).astype(out.dtype)
 
     last = []
-    for n, h, out, target, copy in late:
+    for n, h, target, copy in late:
         copy.wait_recv()
         if n == h:
-            held = out.at[(side, front)[n], target]
+            held = target((side, front)[n], h)
             last.append(sender.start(held, held, names[1 - n]))
     for copy in last:
         copy.wait_recv()
@@ -831,8 +878,9 @@
 
     @pl.when(row == height)
     def _():
-        for o in range(1, nz):
-            spread_copy(o).wait_send()
+        for turn in range(nf):
+            for o in range(1, nz):
+                spread_copy(turn, o).wait_send()
 
 
 def flush_kernel(*refs):
@@ -864,7 +912,8 @@
     piece, thin, wide = half // nz, rank // nf, features // nf
     cols = qu.shape[1] + ku.shape[1]
     coded_rows = 3 * rank + 16
-    count = 80
+    count = 136
+    k_early = early // 16 * K_EARLY_OF_16
     f32, b16 = jnp.float32, jnp.bfloat16
     vmem = pltpu.VMEM
     outs = [vmem(m.shape, f32) for m in (mq, mk, mb)] * 2
@@ -903,10 +952,12 @@
             vmem((nt, 8, 128), f32),
             vmem((early, mq.shape[1]), b16),
             vmem((nf, early, mq.shape[1]), b16),
+            vmem((k_early, mk.shape[1]), b16),
+            vmem((nf, k_early, mk.shape[1]), b16),
             pltpu.SemaphoreType.DMA((count,)),
             pltpu.SemaphoreType.DMA((count,)),
             pltpu.SemaphoreType.DMA((32,)),
-            pltpu.SemaphoreType.DMA((nf + 1,)),
+            pltpu.SemaphoreType.DMA((2 * nf,)),
         ],
         compiler_params=pltpu.CompilerParams(
             collective_id=0, has_side_effects=True, vmem_limit_bytes=VMEM_LIMIT

time: 105 us -> 102 us (0.971)
  the two profiles are of different devices: /device:TPU:27 before, /device:TPU:0 now
where the time goes in v3:
time: 102 us
  Pallas kernels  101 us (99%)
    pallas_call x1, Pallas kernels, fused(): pl.pallas_call(functools.partial(fused_kernel, nf, nt, early), out_shape=...  94 us
    pallas_call x1, Pallas kernels, flushed(): pl.pallas_call(flush_kernel, out_shape=tuple((jax.ShapeDtypeStruct(r.shap...  7.11 us

profile of v3, /device:TPU:0, one launch (start us, length us, event | category | flops | bytes accessed | tf_op | source)
XLA Modules:
  0.0 102.0 jit_solution(9089750861810223268)
XLA Ops:
  0.7 94.0 %shard_map.280 = (f32[1024,512]{1,0:T(8,128)S(1)}, f32[1024,128]{1,0:T(8,128)S(1)}, f32[1024,512]{1,0:T(8,128)S(1)}, f32[1024,512]{1,0:T(8,128)S(1)}, f32[1024,1...) custom-call(bf16[1024,512]{1,0:T(8,128)(2,1)} %x_hbm.1, ...), custom_call_target="tpu_custom_call" | custom-call | tf_op jit(solution)/shard_map/pallas_call | solution.py:923
  94.7 7.1 %shard_map.281 = (f32[1024,512]{1,0:T(8,128)}, f32[1024,128]{1,0:T(8,128)}, f32[1024,512]{1,0:T(8,128)}, f32[1024,512]{1,0:T(8,128)}, f32[1024,128]{1,0:T(8,128)...) custom-call(f32[1024,512]{1,0:T(8,128)S(1)} %get-tuple-element.45.re, ...), custom_call_target="tpu_custom_call" | custom-call | tf_op jit(solution)/shard_map/pallas_call | solution.py:897
